TPU v7x, 32 devices: a whole 2x2x4 slice. The times are simulated.
32 devices in a mesh: sp: 8 (over z, y), tp: 4 (over x, core).
Axes of the slice: x: 2, y: 2, z: 4, core: 2. Of those that a mesh axis runs over, the one named last changes fastest.
Arguments:
- cotangent: bfloat16 [1280, 2048], P('sp'), may hold values from -8 to 8
- saved_input: bfloat16 [1280, 2048], P('sp'), may hold values from -200 to 200
- routes: int32 [1280, 2], P('sp'), may hold values from 0 to 7, all different within a row; in each aligned block of 160 rows (0 to 159, 160 to 319, ...) at most 80 rows name the same one
- route_weight: float32 [1280, 2], P('sp'), may hold values from 0.2 to 1.5
- gate_proj: bfloat16 [8, 2048, 1024], P('sp', None, 'tp'), may hold values from -0.125 to 0.125
- up_proj: bfloat16 [8, 2048, 1024], P('sp', None, 'tp'), may hold values from -0.125 to 0.125
- down_proj: bfloat16 [8, 1024, 2048], P('sp', 'tp'), may hold values from -0.1875 to 0.1875
- out_proj: bfloat16 [2048, 1024], P(None, 'tp'), may hold values from -0.1875 to 0.1875
- conv_input: bfloat16 [1280, 1024], P('sp', 'tp'), may hold values from -6 to 6
- gate_branch: bfloat16 [1280, 1024], P('sp', 'tp'), may hold values from -6 to 6
- conv_taps: bfloat16 [4, 1024], P(None, 'tp'), may hold values from -3 to 3
- recur_map: bfloat16 [2, 16, 64, 64], P(None, 'tp'), may hold values from -0.75 to 0.75
- input_map: bfloat16 [2, 16, 64, 64], P(None, 'tp'), may hold values from -0.75 to 0.75
- decay_param: float32 [2, 1024], P(None, 'tp'), may hold values from 4 to 30
- decay_shift: float32 [2, 1280, 1024], P(None, 'sp', 'tp'), may hold values from -2 to 0, as said below
Outputs:
- grad_gate_proj: float32 [8, 2048, 1024], P('sp', None, 'tp')
- grad_up_proj: float32 [8, 2048, 1024], P('sp', None, 'tp')
- grad_down_proj: float32 [8, 1024, 2048], P('sp', 'tp')
- grad_out_proj: float32 [2048, 1024], P('sp', 'tp')
- grad_conv_input: bfloat16 [1280, 1024], P('sp', 'tp')
- grad_gate_branch: bfloat16 [1280, 1024], P('sp', 'tp')
Inputs may be any that keep to these rules, and one draw needn't show every extreme that they name: Each row names 2 different experts; among the rows of one device no expert is named by more than 80 rows, and in every draw some device routes exactly 80 rows to some expert. `decay_shift`: together with decay_param, -log_decay stays at or above softplus(-decay_param) for every channel and position.
All inputs are finite; a program needn't handle non-finite values.
Results may differ from a plain program's by a relative error of at most 0.013.
Values may be sent and summed in bfloat16 or wider, within the bound.
A program may use at most 128 MiB of HBM per device.

v0:
```python
import jax
import jax.numpy as jnp
from jax import lax
from jax.sharding import PartitionSpec as P

EPS = 1e-06
DECAY_SCALE = 8.0


def with_halo(block, sides, width):
    for axis, dim in sides:
        count = lax.axis_size(axis)
        forward = [(i, i + 1) for i in range(count - 1)]
        backward = [(target, source) for source, target in forward]
        low = lax.ppermute(
            lax.slice_in_dim(block, block.shape[dim] - width, None, axis=dim), axis, forward
        )
        high = lax.ppermute(lax.slice_in_dim(block, 0, width, axis=dim), axis, backward)
        block = jnp.concatenate([low, block, high], axis=dim)
    return block


def prefix(part, axis, combine, identity, reverse):
    count = lax.axis_size(axis)
    place = lax.axis_index(axis)
    ahead = count - 1 - place if reverse else place
    gathered = jax.tree.map(lambda a: lax.all_gather(a, axis), part)
    state = jax.tree.map(lambda a, e: jnp.zeros_like(a) + jnp.asarray(e, a.dtype), part, identity)

    def one(lap, state):
        source = count - 1 - lap if reverse else lap
        return combine(
            state, jax.tree.map(lambda a: lax.dynamic_index_in_dim(a, source, 0, False), gathered)
        )

    return lax.fori_loop(0, ahead, one, state)


def block_matrix(maps):
    heads = maps.shape[0]
    eye = jnp.eye(heads, dtype=jnp.float32)
    full = jnp.einsum("hij,hg->higj", maps.astype(jnp.float32), eye)
    return full.reshape(heads * maps.shape[1], heads * maps.shape[2])


def gate_terms(conv_out, recur_map, input_map, decay_param, decay_shift):
    recur = jax.nn.sigmoid(
        jnp.dot(conv_out, block_matrix(recur_map), precision=lax.Precision.HIGHEST)
    )
    inputs = jax.nn.sigmoid(
        jnp.dot(conv_out, block_matrix(input_map), precision=lax.Precision.HIGHEST)
    )
    log_decay = -DECAY_SCALE * recur * jax.nn.softplus(-decay_param)[None, :] + decay_shift
    decay = jnp.exp(log_decay)
    drive = jnp.sqrt(-jnp.expm1(2.0 * log_decay)) * (inputs * conv_out)
    return (decay, drive)


def link(earlier, later):
    return (earlier[0] * later[0], later[0] * earlier[1] + later[1])


def link_pairs(earlier, later):
    first = link((earlier[0], earlier[1]), (later[0], later[1]))
    second = link((earlier[2], earlier[3]), (later[2], later[3]))
    return first + second


def sweep(coef, drive, reverse):
    return lax.associative_scan(link, (coef, drive), axis=0, reverse=reverse)


def shards(
    cotangent,
    saved_input,
    routes,
    route_weight,
    gate_proj,
    up_proj,
    down_proj,
    out_proj,
    conv_input,
    gate_branch,
    conv_taps,
    recur_map,
    input_map,
    decay_param,
    decay_shift,
):
    length, width = cotangent.shape
    top = routes.shape[1]
    experts = lax.axis_size("sp") * gate_proj.shape[0]
    slots = 4 * length // lax.axis_size("sp")
    inputs32 = saved_input.astype(jnp.float32)
    inv_rms = lax.rsqrt(jnp.mean(inputs32 * inputs32, axis=1, keepdims=True) + EPS)
    normed = inputs32 * inv_rms
    expert_input = normed.astype(jnp.bfloat16)
    scaled = (route_weight[:, :, None] * cotangent.astype(jnp.float32)[:, None, :]).astype(
        jnp.bfloat16
    )
    scaled = scaled.reshape(length * top, width)
    flat_expert = routes.reshape(-1)
    onehot = (flat_expert[:, None] == jnp.arange(experts, dtype=jnp.int32)[None, :]).astype(
        jnp.int32
    )
    earlier_count = jnp.cumsum(onehot, axis=0) - onehot
    rank = jnp.sum(earlier_count * onehot, axis=1)
    target = flat_expert * slots + rank
    token_of = jnp.arange(length * top, dtype=jnp.int32) // top
    fourth = width // lax.axis_size("tp")
    first_col = lax.axis_index("tp") * fourth
    own_scaled = lax.dynamic_slice_in_dim(scaled, first_col, fourth, 1)
    own_input = lax.dynamic_slice_in_dim(expert_input, first_col, fourth, 1)
    send_scaled = jnp.zeros((experts * slots, fourth), jnp.bfloat16).at[target].set(own_scaled)
    send_input = (
        jnp.zeros((experts * slots, fourth), jnp.bfloat16).at[target].set(own_input[token_of])
    )
    part_scaled, part_input = (
        lax.all_to_all(
            send_scaled.reshape(experts, slots, fourth),
            "sp",
            split_axis=0,
            concat_axis=0,
            tiled=True,
        ),
        lax.all_to_all(
            send_input.reshape(experts, slots, fourth),
            "sp",
            split_axis=0,
            concat_axis=0,
            tiled=True,
        ),
    )
    got_scaled, got_input = (
        lax.all_gather(part_scaled, "tp", axis=2, tiled=True),
        lax.all_gather(part_input, "tp", axis=2, tiled=True),
    )
    rows_scaled = got_scaled.reshape(experts * slots, width)
    rows_input = got_input.reshape(experts * slots, width)
    w_gate = gate_proj[0]
    w_up = up_proj[0]
    w_down = down_proj[0]
    gate_pre = jnp.dot(rows_input, w_gate, preferred_element_type=jnp.float32)
    up_pre = jnp.dot(rows_input, w_up, preferred_element_type=jnp.float32)
    gate_sig = jax.nn.sigmoid(gate_pre)
    gate_act = gate_pre * gate_sig
    hidden = (gate_act * up_pre).astype(jnp.bfloat16)
    hidden_grad = lax.dot_general(
        rows_scaled, w_down, (((1,), (1,)), ((), ())), preferred_element_type=jnp.float32
    )
    gate_grad = (hidden_grad * up_pre * gate_sig * (1.0 + gate_pre * (1.0 - gate_sig))).astype(
        jnp.bfloat16
    )
    up_grad = (hidden_grad * gate_act).astype(jnp.bfloat16)
    grad_down = lax.dot_general(
        hidden, rows_scaled, (((0,), (0,)), ((), ())), preferred_element_type=jnp.float32
    )
    grad_gate = lax.dot_general(
        rows_input, gate_grad, (((0,), (0,)), ((), ())), preferred_element_type=jnp.float32
    )
    grad_up = lax.dot_general(
        rows_input, up_grad, (((0,), (0,)), ((), ())), preferred_element_type=jnp.float32
    )
    partial_rows = lax.dot_general(
        gate_grad, w_gate, (((1,), (1,)), ((), ())), preferred_element_type=jnp.float32
    )
    partial_rows = partial_rows + lax.dot_general(
        up_grad, w_up, (((1,), (1,)), ((), ())), preferred_element_type=jnp.float32
    )
    summed = lax.psum(partial_rows.astype(jnp.bfloat16), "tp")
    back = lax.all_to_all(
        summed.reshape(experts, slots, width), "sp", split_axis=0, concat_axis=0, tiled=True
    )
    routed = back.reshape(experts * slots, width)[target].reshape(length, top, width)
    normed_grad = jnp.sum(routed.astype(jnp.float32), axis=1)
    mixed_grad = cotangent.astype(jnp.float32) + inv_rms * (
        normed_grad - normed * jnp.mean(normed_grad * normed, axis=1, keepdims=True)
    )
    mixed_grad_b = mixed_grad.astype(jnp.bfloat16)
    taps32 = conv_taps.astype(jnp.float32)
    padded = with_halo(conv_input, (("sp", 0),), 2)
    conv_out = jnp.zeros((length, padded.shape[1]), jnp.float32)
    for offset in range(taps32.shape[0]):
        conv_out = conv_out + padded[offset : offset + length].astype(jnp.float32) * taps32[offset]
    (coef_f, drive_f), pull_f = jax.vjp(
        lambda value: gate_terms(value, recur_map[0], input_map[0], decay_param[0], decay_shift[0]),
        conv_out,
    )
    (coef_b, drive_b), pull_b = jax.vjp(
        lambda value: gate_terms(value, recur_map[1], input_map[1], decay_param[1], decay_shift[1]),
        conv_out,
    )
    out_grad = jnp.dot(mixed_grad_b, out_proj, preferred_element_type=jnp.float32)
    activated, pull_gelu = jax.vjp(jax.nn.gelu, gate_branch.astype(jnp.float32))
    carried = out_grad * activated
    cum_f, state_f0 = sweep(coef_f, drive_f, False)
    cum_bf, after_b0 = sweep(coef_b, coef_b * carried, False)
    cum_b, state_b0 = sweep(coef_b, drive_b, True)
    cum_fr, after_f0 = sweep(coef_f, coef_f * carried, True)
    ones = jnp.ones((conv_out.shape[1],), jnp.float32)
    zero_filled = jnp.zeros((conv_out.shape[1],), jnp.float32)
    lower = prefix(
        (cum_f[-1], state_f0[-1], cum_bf[-1], after_b0[-1]),
        "sp",
        link_pairs,
        (ones, zero_filled, ones, zero_filled),
        False,
    )
    upper = prefix(
        (cum_b[0], state_b0[0], cum_fr[0], after_f0[0]),
        "sp",
        link_pairs,
        (ones, zero_filled, ones, zero_filled),
        True,
    )
    state_f = state_f0 + cum_f * lower[1][None, :]
    after_b = after_b0 + cum_bf * lower[3][None, :]
    state_b = state_b0 + cum_b * upper[1][None, :]
    after_f = after_f0 + cum_fr * upper[3][None, :]
    adjoint_f = carried + jnp.concatenate([after_f[1:], upper[3][None, :]], axis=0)
    adjoint_b = carried + jnp.concatenate([lower[3][None, :], after_b[:-1]], axis=0)
    prev_f = jnp.concatenate([lower[1][None, :], state_f[:-1]], axis=0)
    next_b = jnp.concatenate([state_b[1:], upper[1][None, :]], axis=0)
    conv_grad = (
        pull_f((adjoint_f * prev_f, adjoint_f))[0] + pull_b((adjoint_b * next_b, adjoint_b))[0]
    )
    states = state_f + state_b
    mixed_out = (activated * states).astype(jnp.bfloat16)
    branch_grad = pull_gelu(out_grad * states)[0].astype(jnp.bfloat16)
    grad_out = lax.psum_scatter(
        lax.dot_general(
            mixed_grad_b, mixed_out, (((0,), (0,)), ((), ())), preferred_element_type=jnp.float32
        ),
        "sp",
        scatter_dimension=0,
        tiled=True,
    )
    grad_pad = with_halo(conv_grad.astype(jnp.bfloat16), (("sp", 0),), 2).astype(conv_grad.dtype)
    input_grad = jnp.zeros((length, conv_grad.shape[1]), jnp.float32)
    for offset in range(taps32.shape[0]):
        input_grad = input_grad + grad_pad[4 - offset : 4 - offset + length] * taps32[offset]
    return (
        grad_gate[None],
        grad_up[None],
        grad_down[None],
        grad_out,
        input_grad.astype(jnp.bfloat16),
        branch_grad,
    )


def solution(mesh):
    in_specs = (
        P("sp", None),
        P("sp", None),
        P("sp", None),
        P("sp", None),
        P("sp", None, "tp"),
        P("sp", None, "tp"),
        P("sp", "tp", None),
        P(None, "tp"),
        P("sp", "tp"),
        P("sp", "tp"),
        P(None, "tp"),
        P(None, "tp", None, None),
        P(None, "tp", None, None),
        P(None, "tp"),
        P(None, "sp", "tp"),
    )
    out_specs = (
        P("sp", None, "tp"),
        P("sp", None, "tp"),
        P("sp", "tp", None),
        P("sp", "tp"),
        P("sp", "tp"),
        P("sp", "tp"),
    )
    return jax.shard_map(shards, mesh=mesh, in_specs=in_specs, out_specs=out_specs, check_vma=False)
```

profile of v0, /device:TPU:0, one launch (start us, length us, event | category | flops | bytes accessed | tf_op | source)
XLA Modules:
  0.0 605.2 jit_solution(16723660355794471832)
XLA Ops:
  13.1 3.4 scatter_custom_fusion
  16.5 24.9 %all_to_all.15 = bf16[8,80,512]{2,1,0:T(8,128)(2,1)} all-to-all(bf16[8,80,512]{2,1,0:T(8,128)(2,1)S(1)} %bitcast.163), channel_id=1, replica_groups=mesh['sp'=8,'tp'=4] {'sp'}, dimensions={0} | all-to-all | bytes 1310720 | tf_op jit(solution)/shard_map/all_to_all | solution.py:126
  41.5 2.8 mul.742
  44.3 4.6 mul.743
  49.2 2.5 scatter_custom_fusion.1
  51.7 20.7 %all_to_all.16 = bf16[8,80,512]{2,1,0:T(8,128)(2,1)} all-to-all(bf16[8,80,512]{2,1,0:T(8,128)(2,1)S(1)} %bitcast.162), channel_id=1, replica_groups=mesh['sp'=8,'tp'=4] {'sp'}, dimensions={0} | all-to-all | bytes 1310720 | tf_op jit(solution)/shard_map/all_to_all | solution.py:119
  73.1 3.6 fusion.17
  78.4 18.4 %all-gather.13.cloned.1.call-done = bf16[8,80,2048]{2,1,0:T(8,128)(2,1)} async-done(((bf16[8,80,512]{2,1,0:T(8,128)(2,1)}), bf16[8,80,2048]{2,1,0:T(8,128)(2,1)}) %all-gather.13.cloned.1.call-update) | async-done | bytes 2621456 | tf_op jit(solution)/shard_map/all_gather | solution.py:135
  96.8 3.4 multiply_convert_fusion.1
  101.1 2.3 add_convert_fusion
  103.5 60.0 %all-reduce.115.cloned.1.call-done = bf16[8,80,2048]{2,1,0:T(8,128)(2,1)} async-done(((bf16[8,80,2048]{2,1,0:T(8,128)(2,1)}), bf16[8,80,2048]{2,1,0:T(8,128)(2,1)}) %all-reduce.115.cloned.1.call-update) | async-done | bytes 2621456 | tf_op jit(solution)/shard_map/psum | solution.py:170
  163.6 5.5 all-to-all-start.2
  169.1 3.9 collective-permute-start
  179.8 2.1 reshape.182
  186.0 4.2 collective-permute-done
  197.4 30.9 %all-to-all-done.2 = bf16[8,80,2048]{2,1,0:T(8,128)(2,1)S(1)} async-done(((bf16[8,80,2048]{2,1,0:T(8,128)(2,1)}), bf16[8,80,2048]{2,1,0:T(8,128)(2,1)S(1)}, u32[]{:S(2)}, u32[]{:S(2)}) %all-to-all-start.2) | async-done | bytes 2621472 | tf_op jit(solution)/shard_map/all_to_all | solution.py:171
  228.3 3.2 gather_fusion
  231.5 4.1 reshape.184
  235.5 5.0 reduce_sum.41
  332.4 22.5 %all-gather.4 = f32[8,1,256]{2,1,0:T(1,128)S(1)} all-gather(f32[1,1,256]{2,1,0:T(1,128)} %add_bitcast_fusion.4), channel_id=1, replica_groups=mesh['sp'=8,'tp'=4] {'sp'}, dimensions={0}, use_global_device_ids=true | all-gather | bytes 9216 | tf_op jit(solution)/shard_map/all_gather | solution.py:27
  354.9 17.1 %all-gather.5 = f32[8,1,256]{2,1,0:T(1,128)S(1)} all-gather(f32[1,1,256]{2,1,0:T(1,128)} %add_bitcast_fusion.3), channel_id=1, replica_groups=mesh['sp'=8,'tp'=4] {'sp'}, dimensions={0}, use_global_device_ids=true | all-gather | bytes 9216 | tf_op jit(solution)/shard_map/all_gather | solution.py:27
  380.0 17.7 %all-gather.6 = f32[8,1,256]{2,1,0:T(1,128)S(1)} all-gather(f32[1,1,256]{2,1,0:T(1,128)S(1)} %add_bitcast_fusion.2), channel_id=1, replica_groups=mesh['sp'=8,'tp'=4] {'sp'}, dimensions={0}, use_global_device_ids=true | all-gather | bytes 9216 | tf_op jit(solution)/shard_map/all_gather | solution.py:27
  398.5 16.9 %all-gather.7 = f32[8,1,256]{2,1,0:T(1,128)S(1)} all-gather(f32[1,1,256]{2,1,0:T(1,128)S(1)} %add_bitcast_fusion.1), channel_id=1, replica_groups=mesh['sp'=8,'tp'=4] {'sp'}, dimensions={0}, use_global_device_ids=true | all-gather | bytes 9216 | tf_op jit(solution)/shard_map/all_gather | solution.py:27
  426.7 17.6 %all-gather = f32[8,1,256]{2,1,0:T(1,128)S(1)} all-gather(f32[1,1,256]{2,1,0:T(1,128)S(1)} %add_bitcast_fusion.8), channel_id=1, replica_groups=mesh['sp'=8,'tp'=4] {'sp'}, dimensions={0}, use_global_device_ids=true | all-gather | bytes 9216 | tf_op jit(solution)/shard_map/all_gather | solution.py:27
  446.5 17.0 %all-gather.1 = f32[8,1,256]{2,1,0:T(1,128)S(1)} all-gather(f32[1,1,256]{2,1,0:T(1,128)S(1)} %add_bitcast_fusion.7), channel_id=1, replica_groups=mesh['sp'=8,'tp'=4] {'sp'}, dimensions={0}, use_global_device_ids=true | all-gather | bytes 9216 | tf_op jit(solution)/shard_map/all_gather | solution.py:27
  480.0 17.6 %all-gather.2 = f32[8,1,256]{2,1,0:T(1,128)S(1)} all-gather(f32[1,1,256]{2,1,0:T(1,128)S(1)} %add_bitcast_fusion.6), channel_id=1, replica_groups=mesh['sp'=8,'tp'=4] {'sp'}, dimensions={0}, use_global_device_ids=true | all-gather | bytes 9216 | tf_op jit(solution)/shard_map/all_gather | solution.py:27
  501.6 17.0 %all-gather.3 = f32[8,1,256]{2,1,0:T(1,128)S(1)} all-gather(f32[1,1,256]{2,1,0:T(1,128)S(1)} %add_bitcast_fusion.5), channel_id=1, replica_groups=mesh['sp'=8,'tp'=4] {'sp'}, dimensions={0}, use_global_device_ids=true | all-gather | bytes 9216 | tf_op jit(solution)/shard_map/all_gather | solution.py:27
  522.4 4.2 convolution_bitcast_fusion.2
  526.7 2.4 convolution_bitcast_fusion
  537.4 5.5 collective-permute-start.2
  542.9 2.3 convolution_bitcast_fusion.1
  546.0 52.5 %reduce-scatter.2.cloned.1.call-done = f32[256,256]{1,0:T(8,128)} async-done(((f32[2048,256]{1,0:T(8,128)}), f32[256,256]{1,0:T(8,128)}) %reduce-scatter.2.cloned.1.call-update) | async-done | bytes 262160 | tf_op jit(solution)/shard_map/reduce_scatter | solution.py:230
  (711 shorter events, 173.3 us)
Async XLA Ops:
  7.2 65.9 %copy-start = (bf16[1,2048,256]{2,1,0:T(8,128)(2,1)S(1)}, bf16[1,2048,256]{2,1,0:T(8,128)(2,1)}, u32[]{:S(2)}) copy-start(bf16[1,2048,256]{2,1,0:T(8,128)(2,1)} %param.23) | copy-start | bytes 3145732
  7.2 65.8 %all-gather.11.cloned.1.call-start = ((), (), s32[]{:S(2)}) async-start(), calls=%async_computation.4 | async-start | bytes 3276800 | tf_op jit(solution)/shard_map/all_gather | solution.py:136
  41.4 55.4 %all-gather.13.cloned.1.call-start = ((), (), s32[]{:S(2)}) async-start(), calls=%async_computation.5 | async-start | bytes 3276800 | tf_op jit(solution)/shard_map/all_gather | solution.py:135
  72.5 91.1 %all-reduce.115.cloned.1.call-start = ((), (), s32[]{:S(2)}) async-start(), calls=%async_computation.6 | async-start | bytes 5242880 | tf_op jit(solution)/shard_map/psum | solution.py:170
  103.5 65.6 %copy-start.38 = (bf16[160,256]{1,0:T(8,128)(2,1)S(1)}, bf16[160,256]{1,0:T(8,128)(2,1)}, u32[]{:S(2)}) copy-start(bf16[160,256]{1,0:T(8,128)(2,1)} %param.27) | copy-start | bytes 245764
  103.5 70.9 %copy-start.61 = (f32[2,256]{1,0:T(2,128)S(1)}, f32[2,256]{1,0:T(2,128)}, u32[]{:S(2)}) copy-start(f32[2,256]{1,0:T(2,128)} %param.32) | copy-start | bytes 6148
  103.5 71.5 %copy-start.53 = (bf16[4,256]{1,0:T(4,128)(2,1)S(1)}, bf16[4,256]{1,0:T(4,128)(2,1)}, u32[]{:S(2)}) copy-start(bf16[4,256]{1,0:T(4,128)(2,1)} %param.29) | copy-start | bytes 6148
  163.6 64.7 %all-to-all-start.2 = ((bf16[8,80,2048]{2,1,0:T(8,128)(2,1)}), bf16[8,80,2048]{2,1,0:T(8,128)(2,1)S(1)}, u32[]{:S(2)}, u32[]{:S(2)}) async-start(bf16[8,80,2048]{2,1,0:T(8,128)(2,1)} %all-reduce.115.cloned.1.call-done), calls=%async_computation.2 | async-start | bytes 5242880 | tf_op jit(solution)/shard_map/all_to_all | solution.py:171
  169.1 429.4 %reduce-scatter.2.cloned.1.call-start = ((), (), s32[]{:S(2)}) async-start(), calls=%async_computation.7 | async-start | bytes 2359296 | tf_op jit(solution)/shard_map/reduce_scatter | solution.py:230
  169.1 21.1 %collective-permute-start = (bf16[2,256]{1,0:T(2,128)(2,1)S(1)}, bf16[2,256]{1,0:T(2,128)(2,1)S(1)}, u32[]{:S(2)}, u32[]{:S(2)}) collective-permute-start(bf16[2,256]{1,0:T(2,128)(2,1)S(1)} %get-tuple-element.334), channel_id=1, source_target_pairs={{0,4},{4,8},{8,12},{12,16},{16,20},{20,24},{24,28},{1,5},{5,9},{9,... | collective-permute-start | bytes 3080 | tf_op jit(solution)/shard_map/ppermute | solution.py:15
  173.0 17.2 %collective-permute-start.1 = (bf16[2,256]{1,0:T(2,128)(2,1)S(1)}, bf16[2,256]{1,0:T(2,128)(2,1)S(1)}, u32[]{:S(2)}, u32[]{:S(2)}) collective-permute-start(bf16[2,256]{1,0:T(2,128)(2,1)S(1)} %get-tuple-element.333), channel_id=1, source_target_pairs={{4,0},{8,4},{12,8},{16,12},{20,16},{24,20},{28,24},{5,1},{9,5},{13... | collective-permute-start | bytes 3080 | tf_op jit(solution)/shard_map/ppermute | solution.py:18
  297.5 74.5 %copy-start.29 = (f32[79,256]{1,0:T(8,128)S(1)}, f32[79,256]{1,0:T(8,128)}, u32[]{:S(2)}) copy-start(f32[79,256]{1,0:T(8,128)} %slice.1206) | copy-start | bytes 242692
  308.4 70.4 %copy-start.36 = (f32[19,256]{1,0:T(8,128)S(1)}, f32[19,256]{1,0:T(8,128)}, u32[]{:S(2)}) copy-start(f32[19,256]{1,0:T(8,128)} %slice.1202) | copy-start | bytes 58372
  308.4 70.4 %copy-start.37 = (f32[19,256]{1,0:T(8,128)S(1)}, f32[19,256]{1,0:T(8,128)}, u32[]{:S(2)}) copy-start(f32[19,256]{1,0:T(8,128)} %slice.1167) | copy-start | bytes 58372
  313.8 65.7 %copy-start.57 = (f32[1,256]{1,0:T(1,128)S(1)}, f32[1,256]{1,0:T(1,128)}, u32[]{:S(2)}) copy-start(f32[1,256]{1,0:T(1,128)} %slice.1353) | copy-start | bytes 3076
  313.8 65.7 %copy-start.32 = (f32[39,256]{1,0:T(8,128)S(1)}, f32[39,256]{1,0:T(8,128)}, u32[]{:S(2)}) copy-start(f32[39,256]{1,0:T(8,128)} %slice.1204) | copy-start | bytes 119812
  313.8 65.7 %copy-start.33 = (f32[39,256]{1,0:T(8,128)S(1)}, f32[39,256]{1,0:T(8,128)}, u32[]{:S(2)}) copy-start(f32[39,256]{1,0:T(8,128)} %slice.1169) | copy-start | bytes 119812
  313.9 65.7 %copy-start.60 = (f32[1,256]{1,0:T(1,128)S(1)}, f32[1,256]{1,0:T(1,128)}, u32[]{:S(2)}) copy-start(f32[1,256]{1,0:T(1,128)} %slice.1352) | copy-start | bytes 3076
  315.3 64.5 %copy-start.59 = (f32[1,256]{1,0:T(1,128)S(1)}, f32[1,256]{1,0:T(1,128)}, u32[]{:S(2)}) copy-start(f32[1,256]{1,0:T(1,128)} %slice.1372) | copy-start | bytes 3076
  328.6 51.3 %copy-start.56 = (f32[1,256]{1,0:T(1,128)S(1)}, f32[1,256]{1,0:T(1,128)}, u32[]{:S(2)}) copy-start(f32[1,256]{1,0:T(1,128)} %get-tuple-element.310) | copy-start | bytes 3076
  379.5 43.5 %copy-start.34 = (f32[19,256]{1,0:T(8,128)S(1)}, f32[19,256]{1,0:T(8,128)}, u32[]{:S(2)}) copy-start(f32[19,256]{1,0:T(8,128)} %slice.986) | copy-start | bytes 58372
  379.7 44.7 %copy-start.30 = (f32[39,256]{1,0:T(8,128)S(1)}, f32[39,256]{1,0:T(8,128)}, u32[]{:S(2)}) copy-start(f32[39,256]{1,0:T(8,128)} %slice.988) | copy-start | bytes 119812
  379.7 44.7 %copy-start.31 = (f32[39,256]{1,0:T(8,128)S(1)}, f32[39,256]{1,0:T(8,128)}, u32[]{:S(2)}) copy-start(f32[39,256]{1,0:T(8,128)} %slice.948) | copy-start | bytes 119812
  379.9 45.3 %copy-start.58 = (f32[1,256]{1,0:T(1,128)S(1)}, f32[1,256]{1,0:T(1,128)}, u32[]{:S(2)}) copy-start(f32[1,256]{1,0:T(1,128)} %slice.1232) | copy-start | bytes 3076
  379.9 46.0 %copy-start.27 = (f32[79,256]{1,0:T(8,128)S(1)}, f32[79,256]{1,0:T(8,128)}, u32[]{:S(2)}) copy-start(f32[79,256]{1,0:T(8,128)} %slice.990) | copy-start | bytes 242692
  379.9 46.0 %copy-start.28 = (f32[79,256]{1,0:T(8,128)S(1)}, f32[79,256]{1,0:T(8,128)}, u32[]{:S(2)}) copy-start(f32[79,256]{1,0:T(8,128)} %slice.942) | copy-start | bytes 242692
  398.5 47.3 %copy-start.15 = (f32[160,256]{1,0:T(8,128)}, f32[160,256]{1,0:T(8,128)S(1)}, u32[]{:S(2)}) copy-start(f32[160,256]{1,0:T(8,128)S(1)} %pad.459) | copy-start | bytes 491524
  416.8 47.3 %copy-start.54 = (f32[2,256]{1,0:T(2,128)S(1)}, f32[2,256]{1,0:T(2,128)}, u32[]{:S(2)}) copy-start(f32[2,256]{1,0:T(2,128)} %slice.1057) | copy-start | bytes 6148
  416.8 47.3 %copy-start.55 = (f32[2,256]{1,0:T(2,128)S(1)}, f32[2,256]{1,0:T(2,128)}, u32[]{:S(2)}) copy-start(f32[2,256]{1,0:T(2,128)} %slice.1056) | copy-start | bytes 6148
  536.0 9.2 %collective-permute-start.3 = (bf16[2,256]{1,0:T(2,128)(2,1)S(1)}, bf16[2,256]{1,0:T(2,128)(2,1)S(1)}, u32[]{:S(2)}, u32[]{:S(2)}) collective-permute-start(bf16[2,256]{1,0:T(2,128)(2,1)S(1)} %get-tuple-element.316), channel_id=1, source_target_pairs={{4,0},{8,4},{12,8},{16,12},{20,16},{24,20},{28,24},{5,1},{9,5},{13... | collective-permute-start | bytes 3080 | tf_op jit(solution)/shard_map/ppermute | solution.py:18
  537.3 61.1 %copy-start.1 = (bf16[1,2048,256]{2,1,0:T(8,128)(2,1)S(1)}, bf16[1,2048,256]{2,1,0:T(8,128)(2,1)}, u32[]{:S(2)}) copy-start(bf16[1,2048,256]{2,1,0:T(8,128)(2,1)} %param.23) | copy-start | bytes 3145732
  537.4 7.8 %collective-permute-start.2 = (bf16[2,256]{1,0:T(2,128)(2,1)S(1)}, bf16[2,256]{1,0:T(2,128)(2,1)S(1)}, u32[]{:S(2)}, u32[]{:S(2)}) collective-permute-start(bf16[2,256]{1,0:T(2,128)(2,1)S(1)} %get-tuple-element.315), channel_id=1, source_target_pairs={{0,4},{4,8},{8,12},{12,16},{16,20},{20,24},{24,28},{1,5},{5,9},{9,... | collective-permute-start | bytes 3080 | tf_op jit(solution)/shard_map/ppermute | solution.py:15
  (47 other events, 377.7 us)
Sparse Core Ops, SparseCore 0:
  41.6 24.1 all-gather.10
  72.6 24.1 all-gather.12
  103.6 59.8 all-reduce.114
  522.5 75.9 reduce-scatter.1
where the time goes:
time: 616 us; the launch traced here: 605 us
  blocking collectives  189 us (31%)
  waiting for transfers between devices  166 us (27%)
  local copies, waits for them, and re-layouts  118 us (19%)
  other arithmetic  64.7 us (11%)
  matrix products  32.2 us (5%)
  starting transfers between devices  18.1 us (3%)
  between operations  16.6 us (3%)
    all_gather x8, blocking collectives, prefix(): gathered = jax.tree.map(lambda a: lax.all_gather(a, axis), part)  143 us
    slice x198, local copies, waits for them, and re-layouts, sweep(): return lax.associative_scan(link, (coef, drive), axis=0, reverse=reverse)  76.2 us
    psum x1, waiting for transfers between devices, shards(): summed = lax.psum(partial_rows.astype(jnp.bfloat16), 'tp')  60 us
    reduce_scatter x1, waiting for transfers between devices, shards(): lax.psum_scatter(lax.dot_general(mixed_grad_b, mixed_out, (((0,), (0,)),...  52.5 us
    all_to_all x1, waiting for transfers between devices, shards(): lax.all_to_all(summed.reshape(experts, slots, width), 'sp', split_axis=0,...  30.9 us
    all_to_all x1, blocking collectives, shards(): lax.all_to_all(send_input.reshape(experts, slots, fourth), 'sp', split_ax...  24.9 us
    concatenate x48, other arithmetic, sweep(): return lax.associative_scan(link, (coef, drive), axis=0, reverse=reverse)  20.9 us
    all_to_all x1, blocking collectives, shards(): lax.all_to_all(send_scaled.reshape(experts, slots, fourth), 'sp', split_a...  20.7 us
  transfers between devices with their start and end apart: 9, of which 5 were waited for; matrix products, arithmetic and copies ran while one was open for 8% of the time, Pallas kernels for 0%

commit v1 on v0

--- a/solution.py
+++ b/solution.py
@@ -167,7 +167,9 @@
     partial_rows = partial_rows + lax.dot_general(
         up_grad, w_up, (((1,), (1,)), ((), ())), preferred_element_type=jnp.float32
     )
-    summed = lax.psum(partial_rows.astype(jnp.bfloat16), "tp")
+    part_2 = partial_rows.astype(jnp.bfloat16)
+    terms = lax.all_gather(part_2, "tp")
+    summed = jnp.sum(terms, axis=0)
     back = lax.all_to_all(
         summed.reshape(experts, slots, width), "sp", split_axis=0, concat_axis=0, tiled=True
     )

time: 616 us -> 635 us (1.031)
  waiting for transfers between devices: 166 us -> 177 us
  other arithmetic: 64.7 us -> 73.4 us
    all_gather x0 -> x1, waiting for transfers between devices: none -> 70.3 us  [shards(): terms = lax.all_gather(part_2, 'tp')]
    psum x1 -> x0, waiting for transfers between devices: 60 us -> none  [shards(): summed = lax.psum(partial_rows.astype(jnp.bfloat16), 'tp')]
    reduce_sum x0 -> x1, other arithmetic: none -> 8.71 us  [shards(): summed = jnp.sum(terms, axis=0)]
where the time goes in v1:
time: 635 us; the launch traced here: 625 us
  blocking collectives  189 us (30%)
  waiting for transfers between devices  177 us (28%)
  local copies, waits for them, and re-layouts  118 us (19%)
  other arithmetic  73.4 us (12%)
  matrix products  32.1 us (5%)
  starting transfers between devices  18.2 us (3%)
  between operations  16.5 us (3%)
    all_gather x8, blocking collectives, prefix(): gathered = jax.tree.map(lambda a: lax.all_gather(a, axis), part)  143 us
    slice x198, local copies, waits for them, and re-layouts, sweep(): return lax.associative_scan(link, (coef, drive), axis=0, reverse=reverse)  76.3 us
    all_gather x1, waiting for transfers between devices, shards(): terms = lax.all_gather(part_2, 'tp')  70.3 us
    reduce_scatter x1, waiting for transfers between devices, shards(): lax.psum_scatter(lax.dot_general(mixed_grad_b, mixed_out, (((0,), (0,)),...  52.3 us
    all_to_all x1, waiting for transfers between devices, shards(): lax.all_to_all(summed.reshape(experts, slots, width), 'sp', split_axis=0,...  30.9 us
    all_to_all x1, blocking collectives, shards(): lax.all_to_all(send_input.reshape(experts, slots, fourth), 'sp', split_ax...  24.9 us
    concatenate x48, other arithmetic, sweep(): return lax.associative_scan(link, (coef, drive), axis=0, reverse=reverse)  20.8 us
    all_to_all x1, blocking collectives, shards(): lax.all_to_all(send_scaled.reshape(experts, slots, fourth), 'sp', split_a...  20.7 us
  transfers between devices with their start and end apart: 9, of which 5 were waited for; matrix products, arithmetic and copies ran while one was open for 8% of the time, Pallas kernels for 0%

profile of v1, /device:TPU:0, one launch (start us, length us, event | category | flops | bytes accessed | tf_op | source)
XLA Modules:
  0.0 624.7 jit_solution(16748103148402855600)
XLA Ops:
  13.1 3.4 scatter_custom_fusion
  16.5 24.9 %all_to_all.15 = bf16[8,80,512]{2,1,0:T(8,128)(2,1)} all-to-all(bf16[8,80,512]{2,1,0:T(8,128)(2,1)S(1)} %bitcast.165), channel_id=1, replica_groups=mesh['sp'=8,'tp'=4] {'sp'}, dimensions={0} | all-to-all | bytes 1310720 | tf_op jit(solution)/shard_map/all_to_all | solution.py:126
  41.5 2.8 mul.742
  44.3 4.6 mul.743
  49.2 2.5 scatter_custom_fusion.1
  51.7 20.7 %all_to_all.16 = bf16[8,80,512]{2,1,0:T(8,128)(2,1)} all-to-all(bf16[8,80,512]{2,1,0:T(8,128)(2,1)S(1)} %bitcast.164), channel_id=1, replica_groups=mesh['sp'=8,'tp'=4] {'sp'}, dimensions={0} | all-to-all | bytes 1310720 | tf_op jit(solution)/shard_map/all_to_all | solution.py:119
  73.0 3.6 fusion.17
  78.3 18.5 %all-gather.15.cloned.1.call-done = bf16[8,80,2048]{2,1,0:T(8,128)(2,1)} async-done(((bf16[8,80,512]{2,1,0:T(8,128)(2,1)}), bf16[8,80,2048]{2,1,0:T(8,128)(2,1)}) %all-gather.15.cloned.1.call-update) | async-done | bytes 2621456 | tf_op jit(solution)/shard_map/all_gather | solution.py:135
  96.8 3.4 multiply_convert_fusion.1
  101.1 2.4 add_convert_fusion
  103.5 70.3 %all-gather.17.cloned.1.call-done = bf16[2560,2048]{1,0:T(8,128)(2,1)} async-done(((bf16[640,2048]{1,0:T(8,128)(2,1)}), bf16[2560,2048]{1,0:T(8,128)(2,1)}) %all-gather.17.cloned.1.call-update) | async-done | bytes 10485776 | tf_op jit(solution)/shard_map/all_gather | solution.py:171
  173.8 8.7 %reduce_sum.53 = bf16[640,2048]{1,0:T(8,128)(2,1)} reduce(bf16[4,640,2048]{2,1,0:T(8,128)(2,1)} %bitcast.163, bf16[]{:T(256)} %constant.111.clone.1), dimensions={0}, to_apply=%region_6.7 | reduce | flops 3932160 | bytes 13107202 | tf_op jit(solution)/shard_map/reduce_sum | solution.py:172
  182.5 5.6 all-to-all-start.2
  188.2 3.9 collective-permute-start
  205.1 4.8 collective-permute-done
  217.2 30.9 %all-to-all-done.2 = bf16[8,80,2048]{2,1,0:T(8,128)(2,1)S(1)} async-done(((bf16[8,80,2048]{2,1,0:T(8,128)(2,1)}), bf16[8,80,2048]{2,1,0:T(8,128)(2,1)S(1)}, u32[]{:S(2)}, u32[]{:S(2)}) %all-to-all-start.2) | async-done | bytes 2621472 | tf_op jit(solution)/shard_map/all_to_all | solution.py:173
  248.0 3.2 gather_fusion
  251.2 4.0 reshape.184
  255.3 5.0 reduce_sum.54
  352.2 22.5 %all-gather.5 = f32[8,1,256]{2,1,0:T(1,128)S(1)} all-gather(f32[1,1,256]{2,1,0:T(1,128)} %add_bitcast_fusion.4), channel_id=1, replica_groups=mesh['sp'=8,'tp'=4] {'sp'}, dimensions={0}, use_global_device_ids=true | all-gather | bytes 9216 | tf_op jit(solution)/shard_map/all_gather | solution.py:27
  374.7 17.1 %all-gather.6 = f32[8,1,256]{2,1,0:T(1,128)S(1)} all-gather(f32[1,1,256]{2,1,0:T(1,128)} %add_bitcast_fusion.3), channel_id=1, replica_groups=mesh['sp'=8,'tp'=4] {'sp'}, dimensions={0}, use_global_device_ids=true | all-gather | bytes 9216 | tf_op jit(solution)/shard_map/all_gather | solution.py:27
  399.7 17.7 %all-gather.7 = f32[8,1,256]{2,1,0:T(1,128)S(1)} all-gather(f32[1,1,256]{2,1,0:T(1,128)S(1)} %add_bitcast_fusion.2), channel_id=1, replica_groups=mesh['sp'=8,'tp'=4] {'sp'}, dimensions={0}, use_global_device_ids=true | all-gather | bytes 9216 | tf_op jit(solution)/shard_map/all_gather | solution.py:27
  418.2 16.9 %all-gather.8 = f32[8,1,256]{2,1,0:T(1,128)S(1)} all-gather(f32[1,1,256]{2,1,0:T(1,128)S(1)} %add_bitcast_fusion.1), channel_id=1, replica_groups=mesh['sp'=8,'tp'=4] {'sp'}, dimensions={0}, use_global_device_ids=true | all-gather | bytes 9216 | tf_op jit(solution)/shard_map/all_gather | solution.py:27
  446.5 17.6 %all-gather.1 = f32[8,1,256]{2,1,0:T(1,128)S(1)} all-gather(f32[1,1,256]{2,1,0:T(1,128)S(1)} %add_bitcast_fusion.8), channel_id=1, replica_groups=mesh['sp'=8,'tp'=4] {'sp'}, dimensions={0}, use_global_device_ids=true | all-gather | bytes 9216 | tf_op jit(solution)/shard_map/all_gather | solution.py:27
  466.3 17.0 %all-gather.2 = f32[8,1,256]{2,1,0:T(1,128)S(1)} all-gather(f32[1,1,256]{2,1,0:T(1,128)S(1)} %add_bitcast_fusion.7), channel_id=1, replica_groups=mesh['sp'=8,'tp'=4] {'sp'}, dimensions={0}, use_global_device_ids=true | all-gather | bytes 9216 | tf_op jit(solution)/shard_map/all_gather | solution.py:27
  499.8 17.6 %all-gather.3 = f32[8,1,256]{2,1,0:T(1,128)S(1)} all-gather(f32[1,1,256]{2,1,0:T(1,128)S(1)} %add_bitcast_fusion.6), channel_id=1, replica_groups=mesh['sp'=8,'tp'=4] {'sp'}, dimensions={0}, use_global_device_ids=true | all-gather | bytes 9216 | tf_op jit(solution)/shard_map/all_gather | solution.py:27
  521.3 17.0 %all-gather.4 = f32[8,1,256]{2,1,0:T(1,128)S(1)} all-gather(f32[1,1,256]{2,1,0:T(1,128)S(1)} %add_bitcast_fusion.5), channel_id=1, replica_groups=mesh['sp'=8,'tp'=4] {'sp'}, dimensions={0}, use_global_device_ids=true | all-gather | bytes 9216 | tf_op jit(solution)/shard_map/all_gather | solution.py:27
  542.1 4.2 convolution_bitcast_fusion.2
  546.4 2.4 convolution_bitcast_fusion
  557.1 5.5 collective-permute-start.2
  562.6 2.3 convolution_bitcast_fusion.1
  565.7 52.3 %reduce-scatter.2.cloned.1.call-done = f32[256,256]{1,0:T(8,128)} async-done(((f32[2048,256]{1,0:T(8,128)}), f32[256,256]{1,0:T(8,128)}) %reduce-scatter.2.cloned.1.call-update) | async-done | bytes 262160 | tf_op jit(solution)/shard_map/reduce_scatter | solution.py:232
  (712 shorter events, 175.3 us)
Async XLA Ops:
  7.2 65.8 %copy-start = (bf16[1,2048,256]{2,1,0:T(8,128)(2,1)S(1)}, bf16[1,2048,256]{2,1,0:T(8,128)(2,1)}, u32[]{:S(2)}) copy-start(bf16[1,2048,256]{2,1,0:T(8,128)(2,1)} %param.23) | copy-start | bytes 3145732
  7.2 65.8 %all-gather.13.cloned.1.call-start = ((), (), s32[]{:S(2)}) async-start(), calls=%async_computation.4 | async-start | bytes 3276800 | tf_op jit(solution)/shard_map/all_gather | solution.py:136
  41.4 55.3 %all-gather.15.cloned.1.call-start = ((), (), s32[]{:S(2)}) async-start(), calls=%async_computation.5 | async-start | bytes 3276800 | tf_op jit(solution)/shard_map/all_gather | solution.py:135
  72.5 101.3 %all-gather.17.cloned.1.call-start = ((), (), s32[]{:S(2)}) async-start(), calls=%async_computation.7 | async-start | bytes 13107200 | tf_op jit(solution)/shard_map/all_gather | solution.py:171
  182.5 65.5 %all-to-all-start.2 = ((bf16[8,80,2048]{2,1,0:T(8,128)(2,1)}), bf16[8,80,2048]{2,1,0:T(8,128)(2,1)S(1)}, u32[]{:S(2)}, u32[]{:S(2)}) async-start(bf16[8,80,2048]{2,1,0:T(8,128)(2,1)} %bitcast.162), calls=%async_computation.2 | async-start | bytes 5242880 | tf_op jit(solution)/shard_map/all_to_all | solution.py:173
  188.1 429.8 %reduce-scatter.2.cloned.1.call-start = ((), (), s32[]{:S(2)}) async-start(), calls=%async_computation.6 | async-start | bytes 2359296 | tf_op jit(solution)/shard_map/reduce_scatter | solution.py:232
  188.2 21.7 %collective-permute-start = (bf16[2,256]{1,0:T(2,128)(2,1)S(1)}, bf16[2,256]{1,0:T(2,128)(2,1)S(1)}, u32[]{:S(2)}, u32[]{:S(2)}) collective-permute-start(bf16[2,256]{1,0:T(2,128)(2,1)S(1)} %get-tuple-element.334), channel_id=1, source_target_pairs={{0,4},{4,8},{8,12},{12,16},{16,20},{20,24},{24,28},{1,5},{5,9},{9,... | collective-permute-start | bytes 3080 | tf_op jit(solution)/shard_map/ppermute | solution.py:15
  192.1 17.8 %collective-permute-start.1 = (bf16[2,256]{1,0:T(2,128)(2,1)S(1)}, bf16[2,256]{1,0:T(2,128)(2,1)S(1)}, u32[]{:S(2)}, u32[]{:S(2)}) collective-permute-start(bf16[2,256]{1,0:T(2,128)(2,1)S(1)} %get-tuple-element.333), channel_id=1, source_target_pairs={{4,0},{8,4},{12,8},{16,12},{20,16},{24,20},{28,24},{5,1},{9,5},{13... | collective-permute-start | bytes 3080 | tf_op jit(solution)/shard_map/ppermute | solution.py:18
  317.3 74.5 %copy-start.29 = (f32[79,256]{1,0:T(8,128)S(1)}, f32[79,256]{1,0:T(8,128)}, u32[]{:S(2)}) copy-start(f32[79,256]{1,0:T(8,128)} %slice.1206) | copy-start | bytes 242692
  328.5 70.0 %copy-start.36 = (f32[19,256]{1,0:T(8,128)S(1)}, f32[19,256]{1,0:T(8,128)}, u32[]{:S(2)}) copy-start(f32[19,256]{1,0:T(8,128)} %slice.1202) | copy-start | bytes 58372
  328.5 70.0 %copy-start.37 = (f32[19,256]{1,0:T(8,128)S(1)}, f32[19,256]{1,0:T(8,128)}, u32[]{:S(2)}) copy-start(f32[19,256]{1,0:T(8,128)} %slice.1167) | copy-start | bytes 58372
  333.7 65.5 %copy-start.57 = (f32[1,256]{1,0:T(1,128)S(1)}, f32[1,256]{1,0:T(1,128)}, u32[]{:S(2)}) copy-start(f32[1,256]{1,0:T(1,128)} %slice.1353) | copy-start | bytes 3076
  333.8 65.5 %copy-start.32 = (f32[39,256]{1,0:T(8,128)S(1)}, f32[39,256]{1,0:T(8,128)}, u32[]{:S(2)}) copy-start(f32[39,256]{1,0:T(8,128)} %slice.1204) | copy-start | bytes 119812
  333.8 65.5 %copy-start.33 = (f32[39,256]{1,0:T(8,128)S(1)}, f32[39,256]{1,0:T(8,128)}, u32[]{:S(2)}) copy-start(f32[39,256]{1,0:T(8,128)} %slice.1169) | copy-start | bytes 119812
  333.8 65.5 %copy-start.60 = (f32[1,256]{1,0:T(1,128)S(1)}, f32[1,256]{1,0:T(1,128)}, u32[]{:S(2)}) copy-start(f32[1,256]{1,0:T(1,128)} %slice.1352) | copy-start | bytes 3076
  335.3 64.3 %copy-start.59 = (f32[1,256]{1,0:T(1,128)S(1)}, f32[1,256]{1,0:T(1,128)}, u32[]{:S(2)}) copy-start(f32[1,256]{1,0:T(1,128)} %slice.1372) | copy-start | bytes 3076
  348.4 51.2 %copy-start.56 = (f32[1,256]{1,0:T(1,128)S(1)}, f32[1,256]{1,0:T(1,128)}, u32[]{:S(2)}) copy-start(f32[1,256]{1,0:T(1,128)} %get-tuple-element.310) | copy-start | bytes 3076
  397.8 42.9 %copy-start.40 = (f32[9,256]{1,0:T(8,128)S(1)}, f32[9,256]{1,0:T(8,128)}, u32[]{:S(2)}) copy-start(f32[9,256]{1,0:T(8,128)} %slice.984) | copy-start | bytes 27652
  399.2 43.6 %copy-start.34 = (f32[19,256]{1,0:T(8,128)S(1)}, f32[19,256]{1,0:T(8,128)}, u32[]{:S(2)}) copy-start(f32[19,256]{1,0:T(8,128)} %slice.986) | copy-start | bytes 58372
  399.3 43.6 %copy-start.35 = (f32[19,256]{1,0:T(8,128)S(1)}, f32[19,256]{1,0:T(8,128)}, u32[]{:S(2)}) copy-start(f32[19,256]{1,0:T(8,128)} %slice.954) | copy-start | bytes 58372
  399.4 44.9 %copy-start.30 = (f32[39,256]{1,0:T(8,128)S(1)}, f32[39,256]{1,0:T(8,128)}, u32[]{:S(2)}) copy-start(f32[39,256]{1,0:T(8,128)} %slice.988) | copy-start | bytes 119812
  399.4 44.9 %copy-start.31 = (f32[39,256]{1,0:T(8,128)S(1)}, f32[39,256]{1,0:T(8,128)}, u32[]{:S(2)}) copy-start(f32[39,256]{1,0:T(8,128)} %slice.948) | copy-start | bytes 119812
  399.6 45.4 %copy-start.58 = (f32[1,256]{1,0:T(1,128)S(1)}, f32[1,256]{1,0:T(1,128)}, u32[]{:S(2)}) copy-start(f32[1,256]{1,0:T(1,128)} %slice.1232) | copy-start | bytes 3076
  399.6 46.1 %copy-start.27 = (f32[79,256]{1,0:T(8,128)S(1)}, f32[79,256]{1,0:T(8,128)}, u32[]{:S(2)}) copy-start(f32[79,256]{1,0:T(8,128)} %slice.990) | copy-start | bytes 242692
  399.7 46.1 %copy-start.28 = (f32[79,256]{1,0:T(8,128)S(1)}, f32[79,256]{1,0:T(8,128)}, u32[]{:S(2)}) copy-start(f32[79,256]{1,0:T(8,128)} %slice.942) | copy-start | bytes 242692
  418.2 47.5 %copy-start.15 = (f32[160,256]{1,0:T(8,128)}, f32[160,256]{1,0:T(8,128)S(1)}, u32[]{:S(2)}) copy-start(f32[160,256]{1,0:T(8,128)S(1)} %pad.459) | copy-start | bytes 491524
  436.5 47.4 %copy-start.54 = (f32[2,256]{1,0:T(2,128)S(1)}, f32[2,256]{1,0:T(2,128)}, u32[]{:S(2)}) copy-start(f32[2,256]{1,0:T(2,128)} %slice.1057) | copy-start | bytes 6148
  436.5 47.4 %copy-start.55 = (f32[2,256]{1,0:T(2,128)S(1)}, f32[2,256]{1,0:T(2,128)}, u32[]{:S(2)}) copy-start(f32[2,256]{1,0:T(2,128)} %slice.1056) | copy-start | bytes 6148
  495.3 43.1 %copy-start.17 = (f32[160,256]{1,0:T(8,128)}, f32[160,256]{1,0:T(8,128)S(1)}, u32[]{:S(2)}) copy-start(f32[160,256]{1,0:T(8,128)S(1)} %pad.390) | copy-start | bytes 491524
  555.7 9.2 %collective-permute-start.3 = (bf16[2,256]{1,0:T(2,128)(2,1)S(1)}, bf16[2,256]{1,0:T(2,128)(2,1)S(1)}, u32[]{:S(2)}, u32[]{:S(2)}) collective-permute-start(bf16[2,256]{1,0:T(2,128)(2,1)S(1)} %get-tuple-element.316), channel_id=1, source_target_pairs={{4,0},{8,4},{12,8},{16,12},{20,16},{24,20},{28,24},{5,1},{9,5},{13... | collective-permute-start | bytes 3080 | tf_op jit(solution)/shard_map/ppermute | solution.py:18
  557.0 61.0 %copy-start.1 = (bf16[1,2048,256]{2,1,0:T(8,128)(2,1)S(1)}, bf16[1,2048,256]{2,1,0:T(8,128)(2,1)}, u32[]{:S(2)}) copy-start(bf16[1,2048,256]{2,1,0:T(8,128)(2,1)} %param.23) | copy-start | bytes 3145732
  557.1 7.8 %collective-permute-start.2 = (bf16[2,256]{1,0:T(2,128)(2,1)S(1)}, bf16[2,256]{1,0:T(2,128)(2,1)S(1)}, u32[]{:S(2)}, u32[]{:S(2)}) collective-permute-start(bf16[2,256]{1,0:T(2,128)(2,1)S(1)} %get-tuple-element.315), channel_id=1, source_target_pairs={{0,4},{4,8},{8,12},{12,16},{16,20},{20,24},{24,28},{1,5},{5,9},{9,... | collective-permute-start | bytes 3080 | tf_op jit(solution)/shard_map/ppermute | solution.py:15
  (47 other events, 279.2 us)
Sparse Core Ops, SparseCore 0:
  41.6 24.1 all-gather.12
  72.6 24.1 all-gather.14
  103.6 70.1 all-gather.16
  542.2 75.7 reduce-scatter.1
